TPU v7x, 32 devices: a whole 2x2x4 slice. The times are simulated.
32 devices in a mesh: ep: 8 (over z, y), tp: 4 (over x, core).
Axes of the slice: x: 2, y: 2, z: 4, core: 2. Of those that a mesh axis runs over, the one named last changes fastest.
Arguments:
- tokens: bfloat16 [64, 2048], P('ep'), may hold values from -4 to 4
- w_query: bfloat16 [2048, 1024], P(None, 'tp'), may hold values from -0.125 to 0.125
- w_key: bfloat16 [2048, 1024], P(None, 'tp'), may hold values from -0.125 to 0.125
- w_value: bfloat16 [2048, 1024], P(None, 'tp'), may hold values from -0.125 to 0.125
- w_outgate: bfloat16 [2048, 1024], P(None, 'tp'), may hold values from -0.125 to 0.125
- w_igate: bfloat16 [2048, 4], P(None, 'tp'), may hold values from -0.125 to 0.125
- w_fgate: bfloat16 [2048, 4], P(None, 'tp'), may hold values from -0.125 to 0.125
- forget_bias: float32 [4], P('tp'), may hold values from -1 to 5
- w_out: bfloat16 [1024, 2048], P('tp'), may hold values from -0.1875 to 0.1875
- gain_mix: float32 [2048], replicated, may hold values from 0.1 to 1.9
- gain_moe: float32 [2048], replicated, may hold values from 0.1 to 1.9
- memory: float32 [64, 4, 256, 256], P('ep', 'tp'), may hold values from -0.4 to 0.4
- normalizer: float32 [64, 4, 256], P('ep', 'tp'), may hold values from -0.8 to 0.8
- stabilizer: float32 [64, 4], P('ep', 'tp'), may hold values from 0 to 2
- expert_gate: bfloat16 [8, 2048, 512], P('ep', None, 'tp'), may hold values from -0.125 to 0.125
- expert_up: bfloat16 [8, 2048, 512], P('ep', None, 'tp'), may hold values from -0.125 to 0.125
- expert_down: bfloat16 [8, 512, 2048], P('ep', 'tp'), may hold values from -1 to 1
- routes: int32 [64, 4], P('ep'), may hold values from 0 to 7, all different within a row; in each aligned block of 8 rows (0 to 7, 8 to 15, ...) at most 8 rows name the same one
- route_weight: float32 [64, 4], P('ep'), may hold values from 0.2 to 1
Outputs:
- output: bfloat16 [64, 2048], P('ep', 'tp')
- memory_next: float32 [64, 4, 256, 256], P('ep', 'tp')
- norm_next: float32 [64, 4, 256], P('ep', 'tp')
- stabilizer_next: float32 [64, 4], P('ep', 'tp')
Inputs may be any that keep to these rules, and one draw needn't show every extreme that they name: `routes`: each row names 4 different experts. Among the 8 rows of one device (aligned blocks), no expert is named more than 8 times, a bound that some block reaches.
All inputs are finite; a program needn't handle non-finite values.
Results may differ from a plain program's by a relative error of at most 0.029.
Values may be sent and summed in bfloat16 or wider, within the bound.
A program may use at most 64 MiB of HBM per device.

v0:
```python
import math

import jax
import jax.numpy as jnp
from jax import lax
from jax.sharding import PartitionSpec as P


def layer_norm(row_data, gain_vec):
    values = row_data.astype(jnp.float32)
    row_mean = jnp.mean(values, -1, keepdims=True)
    centered = values - row_mean
    variance = jnp.mean(centered * centered, -1, keepdims=True)
    return centered * lax.rsqrt(variance + 1e-05) * gain_vec


def slot_targets(routes, experts, capacity):
    flat_routes = routes.reshape(-1)
    onehot = (flat_routes[:, None] == jnp.arange(experts, dtype=jnp.int32)[None, :]).astype(
        jnp.int32
    )
    before = jnp.cumsum(onehot, axis=0) - onehot
    slot_index = jnp.sum(before * onehot, axis=1)
    return flat_routes * capacity + slot_index


def shards(
    tokens,
    w_query,
    w_key,
    w_value,
    w_outgate,
    w_igate,
    w_fgate,
    forget_bias,
    w_out,
    gain_mix,
    gain_moe,
    memory,
    normalizer,
    stabilizer,
    expert_gate,
    expert_up,
    expert_down,
    routes,
    route_weight,
):
    seq_rows = tokens.shape[0]
    model_width = tokens.shape[1]
    head_count = memory.shape[1]
    head_size = memory.shape[2]
    head_cols = head_count * head_size
    normed = layer_norm(tokens, gain_mix).astype(jnp.bfloat16)
    gate_in = jnp.dot(normed, w_igate, preferred_element_type=jnp.float32)
    gate_forget = jnp.dot(normed, w_fgate, preferred_element_type=jnp.float32)
    weights = (w_query, w_key, w_value, w_outgate)
    projected = jnp.concatenate(
        [jnp.dot(normed, weight, preferred_element_type=jnp.float32) for weight in weights], axis=1
    )
    rounded = projected.astype(jnp.bfloat16).reshape(seq_rows, 4, head_count, head_size)
    queries = rounded[:, 0].astype(jnp.float32)
    keys_scaled = rounded[:, 1].astype(jnp.float32) / math.sqrt(head_size)
    values_rows = rounded[:, 2].astype(jnp.float32)
    out_gate = rounded[:, 3].astype(jnp.float32)
    log_forget = jax.nn.log_sigmoid(gate_forget + forget_bias)
    stabilizer_next = jnp.maximum(log_forget + stabilizer, gate_in)
    keep_rate = jnp.exp(log_forget + stabilizer - stabilizer_next)
    admit_rate = jnp.exp(gate_in - stabilizer_next)
    memory_next = (
        keep_rate[:, :, None, None] * memory
        + admit_rate[:, :, None, None] * keys_scaled[:, :, :, None] * values_rows[:, :, None, :]
    )
    norm_next = keep_rate[:, :, None] * normalizer + admit_rate[:, :, None] * keys_scaled
    numerator = jnp.einsum("shk,shkv->shv", queries, memory_next, precision=lax.Precision.HIGHEST)
    denominator = jnp.sum(queries * norm_next, axis=-1)
    readout = numerator / jnp.maximum(jnp.abs(denominator), jnp.exp(-stabilizer_next))[:, :, None]
    mixed = (jax.nn.sigmoid(out_gate) * readout).astype(jnp.bfloat16).reshape(seq_rows, head_cols)
    head_part = jnp.dot(mixed, w_out, preferred_element_type=jnp.float32).astype(jnp.bfloat16)
    summed = lax.psum(head_part, "tp").astype(jnp.float32)
    residual = tokens.astype(jnp.float32) + summed
    expert_in = layer_norm(residual, gain_moe).astype(jnp.bfloat16)
    top_count = routes.shape[1]
    local_experts = expert_gate.shape[0]
    expert_count = local_experts * lax.axis_size("ep")
    capacity = max(2, 2 * seq_rows * top_count // expert_count)
    target = slot_targets(routes, expert_count, capacity)
    outbound = (
        jnp.zeros((expert_count * capacity, model_width), jnp.bfloat16)
        .at[target]
        .set(jnp.repeat(expert_in, top_count, axis=0))
    )
    outbound = outbound.reshape(expert_count, capacity, model_width)
    quarter = model_width // lax.axis_size("tp")
    arrived = lax.all_to_all(outbound, "ep", split_axis=0, concat_axis=0, tiled=True)
    slot_count = arrived.shape[1]
    grouped = arrived.reshape(-1, local_experts, slot_count, model_width)
    gate_part = jnp.einsum(
        "aecd,edf->aecf", grouped, expert_gate, preferred_element_type=jnp.float32
    )
    up_part = jnp.einsum("aecd,edf->aecf", grouped, expert_up, preferred_element_type=jnp.float32)
    hidden = (jax.nn.silu(gate_part) * up_part).astype(jnp.bfloat16)
    partial_value, slot_count = (
        jnp.einsum("aecf,efd->aecd", hidden, expert_down, preferred_element_type=jnp.float32),
        slot_count,
    )
    reduced = lax.psum_scatter(partial_value, "tp", scatter_dimension=3, tiled=True).astype(
        jnp.bfloat16
    )
    reduced = reduced.reshape(-1, slot_count, reduced.shape[3])
    returned = lax.all_to_all(reduced, "ep", split_axis=0, concat_axis=0, tiled=True)
    picked = jnp.take(returned.reshape(expert_count * capacity, quarter), target, axis=0).reshape(
        seq_rows, top_count, quarter
    )
    combined = jnp.sum(route_weight[:, :, None] * picked.astype(jnp.float32), axis=1)
    own_cols = lax.dynamic_slice_in_dim(residual, lax.axis_index("tp") * quarter, quarter, 1)
    output = (own_cols + combined).astype(jnp.bfloat16)
    return (output, memory_next, norm_next, stabilizer_next)


def solution(mesh):
    return jax.shard_map(
        shards,
        mesh=mesh,
        in_specs=(
            P("ep", None),
            P(None, "tp"),
            P(None, "tp"),
            P(None, "tp"),
            P(None, "tp"),
            P(None, "tp"),
            P(None, "tp"),
            P("tp"),
            P("tp", None),
            P(),
            P(),
            P("ep", "tp", None, None),
            P("ep", "tp", None),
            P("ep", "tp"),
            P("ep", None, "tp"),
            P("ep", None, "tp"),
            P("ep", "tp", None),
            P("ep", None),
            P("ep", None),
        ),
        out_specs=(P("ep", "tp"), P("ep", "tp", None, None), P("ep", "tp", None), P("ep", "tp")),
        check_vma=False,
    )
```

profile of v0, /device:TPU:0, one launch (start us, length us, event | category | flops | bytes accessed | tf_op | source)
XLA Modules:
  0.0 94.1 jit_solution(10027938302184542748)
XLA Ops:
  7.2 0.9 copy.30
  8.2 1.0 %convert_reduce_fusion = f32[8]{0:T(128)S(1)} fusion(bf16[8,2048]{1,0:T(8,128)(2,1)} %param.19), kind=kLoop, calls=%fused_computation.36 | loop fusion | flops 32760 | bytes 32800 | tf_op jit(solution)/shard_map/reduce_sum | solution.py:11
  9.3 1.0 %fusion.24 = f32[8]{0:T(128)S(1)} fusion(bf16[8,2048]{1,0:T(8,128)(2,1)} %param.19, f32[8]{0:T(128)S(1)} %broadcast_multiply_fusion.3), kind=kLoop, calls=%fused_computation.39 | loop fusion | flops 65528 | bytes 32832 | tf_op jit(solution)/shard_map/reduce_sum | solution.py:13
  10.9 0.8 fusion.26
  11.7 0.8 convolution_bitcast_fusion.3
  12.6 0.8 exponential_bitcast_fusion
  13.4 1.5 %fusion.5 = f32[8,256]{1,0:T(8,128)S(1)} fusion(bf16[8,2048]{1,0:T(8,128)(2,1)S(1)} %fusion.26, bf16[2048,256]{1,0:T(8,128)(2,1)} %param.22), kind=kOutput, calls=%fused_computation.13 | convolution fusion | flops 8392704 | bytes 1089536 | tf_op jit(solution)/shard_map/dot_general | solution.py:58
  14.9 1.4 %broadcast_multiply_fusion = (f32[8,256]{1,0:T(8,128)S(1)}, f32[8,256]{1,0:T(8,128)S(1)}) fusion(f32[8]{0:T(128)S(1)} %multiply_bitcast_fusion, bf16[8,2048]{1,0:T(8,128)(2,1)S(1)} %fusion.26, bf16[2048,256]{1,0:T(8,128)(2,1)} %param.21), kind=kOutput, calls=%fused_computation.68 | convolution fusion | flops 8394752 | bytes 1097760 | tf_op jit(solution)/shard_map/dot_general | solution.py:58
  16.4 0.4 fusion.34
  16.8 0.5 multiply_add_fusion
  17.3 0.8 fusion
  18.1 2.0 %convolution_convert_fusion = bf16[8,2048]{1,0:T(8,128)(2,1)S(1)} fusion(bf16[256,2048]{1,0:T(8,128)(2,1)S(1)} %copy-done, bf16[8,2048]{1,0:T(8,128)(2,1)S(1)} %fusion.26, bf16[2048,256]{1,0:T(8,128)(2,1)} %param.23, f32[8,1,256]{2,1,0:T(1,128)S(1)} %fusion, f32[8]{0:T(128)S(1)} %fusion.42), kind=kOutput, calls=%fused_computation.3 | convolution fusion | flops 16809984 | bytes 2170912 | tf_op jit(solution)/shard_map/dot_general | solution.py:78
  20.1 12.9 %psum.7 = bf16[8,2048]{1,0:T(8,128)(2,1)S(1)} all-reduce(bf16[8,2048]{1,0:T(8,128)(2,1)S(1)} %convolution_convert_fusion), channel_id=1, replica_groups=mesh['ep'=8,'tp'=4] {'tp'}, use_global_device_ids=true, to_apply=%region_3.4 | all-reduce | flops 16384 | bytes 65536 | tf_op jit(solution)/shard_map/psum | solution.py:79
  34.0 0.9 scatter_custom_fusion
  34.9 13.9 %all_to_all.10 = bf16[8,8,2048]{2,1,0:T(8,128)(2,1)S(1)} all-to-all(bf16[8,8,2048]{2,1,0:T(8,128)(2,1)S(1)} %bitcast.115), channel_id=1, replica_groups=mesh['ep'=8,'tp'=4] {'ep'}, dimensions={0} | all-to-all | bytes 524288 | tf_op jit(solution)/shard_map/all_to_all | solution.py:94
  48.7 1.3 %convolution_bitcast_fusion.2 = f32[8,1,8,128]{3,2,0,1:T(8,128)S(1)} fusion(bf16[8,8,2048]{2,1,0:T(8,128)(2,1)S(1)} %all_to_all.10, bf16[1,2048,128]{2,1,0:T(8,128)(2,1)} %param.33), kind=kOutput, calls=%fused_computation.9 | convolution fusion | flops 33554432 | bytes 819200 | tf_op jit(solution)/shard_map/aecd,edf->aecf/dot_general | solution.py:97
  50.0 1.2 %convolution_bitcast_fusion = f32[8,1,8,2048]{3,2,0,1:T(8,128)} fusion(bf16[8,8,2048]{2,1,0:T(8,128)(2,1)S(1)} %all_to_all.10, bf16[1,128,2048]{2,1,0:T(8,128)(2,1)S(1)} %copy-done.5, bf16[1,2048,128]{2,1,0:T(8,128)(2,1)S(1)} %copy-done.6, f32[8,1,8,128]{3,2,0,1:T(8,128)S(1)} %convolution_bitcast_fusion.2), kind=kOutput, calls=%fused_computation.2 | convolution fusion | flops 67158016 | bytes 1867776 | tf_op jit(solution)/shard_map/aecf,efd->aecd/dot_general | solution.py:103
  51.3 20.7 %reduce-scatter.2.cloned.1.call-done = f32[8,1,8,512]{3,2,0,1:T(8,128)} async-done(((f32[8,1,8,2048]{3,2,0,1:T(8,128)}), f32[8,1,8,512]{3,2,0,1:T(8,128)}) %reduce-scatter.2.cloned.1.call-update) | async-done | bytes 131088 | tf_op jit(solution)/shard_map/reduce_scatter | solution.py:106
  72.0 1.5 %convert_bitcast_fusion = bf16[8,8,512]{2,1,0:T(8,128)(2,1)} fusion(f32[8,1,8,512]{3,2,0,1:T(8,128)} %reduce-scatter.2.cloned.1.call-done), kind=kLoop, calls=%fused_computation.43 | loop fusion | flops 32768 | bytes 196608 | tf_op jit(solution)/shard_map/reshape | solution.py:109
  73.5 5.5 %all-to-all-start.1 = ((bf16[8,8,512]{2,1,0:T(8,128)(2,1)}), bf16[8,8,512]{2,1,0:T(8,128)(2,1)S(1)}, u32[]{:S(2)}, u32[]{:S(2)}) async-start(bf16[8,8,512]{2,1,0:T(8,128)(2,1)} %convert_bitcast_fusion), calls=%async_computation.2 | async-start | bytes 131072 | tf_op jit(solution)/shard_map/all_to_all | solution.py:110
  79.1 0.6 copy.32
  79.7 6.2 %all-to-all-done.1 = bf16[8,8,512]{2,1,0:T(8,128)(2,1)S(1)} async-done(((bf16[8,8,512]{2,1,0:T(8,128)(2,1)}), bf16[8,8,512]{2,1,0:T(8,128)(2,1)S(1)}, u32[]{:S(2)}, u32[]{:S(2)}) %all-to-all-start.1) | async-done | bytes 65568 | tf_op jit(solution)/shard_map/all_to_all | solution.py:110
  85.9 0.6 gather_fusion
  86.7 0.6 add_convert_fusion
  (48 shorter events, 1.5 us)
Async XLA Ops:
  7.2 11.0 %copy-start = (bf16[256,2048]{1,0:T(8,128)(2,1)S(1)}, bf16[256,2048]{1,0:T(8,128)(2,1)}, u32[]{:S(2)}) copy-start(bf16[256,2048]{1,0:T(8,128)(2,1)} %param.27) | copy-start | bytes 3145732
  7.2 9.2 %copy-start.4 = (bf16[2048,256]{1,0:T(8,128)(2,1)S(1)}, bf16[2048,256]{1,0:T(8,128)(2,1)}, u32[]{:S(2)}) copy-start(bf16[2048,256]{1,0:T(8,128)(2,1)} %param.20) | copy-start | bytes 3145732
  7.2 9.2 %copy-start.7 = (f32[8,1,256]{2,1,0:T(1,128)S(1)}, f32[8,1,256]{2,1,0:T(1,128)}, u32[]{:S(2)}) copy-start(f32[8,1,256]{2,1,0:T(1,128)} %param.31) | copy-start | bytes 24580
  7.2 64.8 %reduce-scatter.2.cloned.1.call-start = ((), (), s32[]{:S(2)}) async-start(), calls=%async_computation.3 | async-start | bytes 655360 | tf_op jit(solution)/shard_map/reduce_scatter | solution.py:106
  8.2 8.6 %copy-start.2 = (f32[8,1,256,256]{3,2,1,0:T(8,128)S(1)}, f32[8,1,256,256]{3,2,1,0:T(8,128)}, u32[]{:S(2)}) copy-start(f32[8,1,256,256]{3,2,1,0:T(8,128)} %param.30) | copy-start | bytes 6291460
  13.4 3.8 %copy-start.10 = (f32[8,1]{0,1:T(1,128)}, f32[8,1]{0,1:T(1,128)S(1)}, u32[]{:S(2)}) copy-start(f32[8,1]{0,1:T(1,128)S(1)} %get-tuple-element.15) | copy-start | bytes 100
  17.3 2.8 %copy-start.1 = (f32[8,1,256,256]{3,2,1,0:T(8,128)}, f32[8,1,256,256]{3,2,1,0:T(8,128)S(1)}, u32[]{:S(2)}) copy-start(f32[8,1,256,256]{3,2,1,0:T(8,128)S(1)} %multiply_add_fusion) | copy-start | bytes 6291460
  17.3 15.7 %copy-start.3 = (bf16[8,2048]{1,0:T(8,128)(2,1)S(1)}, bf16[8,2048]{1,0:T(8,128)(2,1)}, u32[]{:S(2)}) copy-start(bf16[8,2048]{1,0:T(8,128)(2,1)} %param.19) | copy-start | bytes 98308
  17.3 16.1 %copy-start.8 = (f32[2048]{0:T(1024)S(1)}, f32[2048]{0:T(1024)}, u32[]{:S(2)}) copy-start(f32[2048]{0:T(1024)} %param.29) | copy-start | bytes 24580
  33.0 17.0 %copy-start.5 = (bf16[1,128,2048]{2,1,0:T(8,128)(2,1)S(1)}, bf16[1,128,2048]{2,1,0:T(8,128)(2,1)}, u32[]{:S(2)}) copy-start(bf16[1,128,2048]{2,1,0:T(8,128)(2,1)} %param.35) | copy-start | bytes 1572868
  33.0 17.0 %copy-start.6 = (bf16[1,2048,128]{2,1,0:T(8,128)(2,1)S(1)}, bf16[1,2048,128]{2,1,0:T(8,128)(2,1)}, u32[]{:S(2)}) copy-start(bf16[1,2048,128]{2,1,0:T(8,128)(2,1)} %param.34) | copy-start | bytes 1572868
  34.9 44.2 %copy-start.9 = (f32[8,4]{0,1:T(4,128)S(1)}, f32[8,4]{0,1:T(4,128)}, u32[]{:S(2)}) copy-start(f32[8,4]{0,1:T(4,128)} %param.37) | copy-start | bytes 388
  73.5 12.4 %all-to-all-start.1 = ((bf16[8,8,512]{2,1,0:T(8,128)(2,1)}), bf16[8,8,512]{2,1,0:T(8,128)(2,1)S(1)}, u32[]{:S(2)}, u32[]{:S(2)}) async-start(bf16[8,8,512]{2,1,0:T(8,128)(2,1)} %convert_bitcast_fusion), calls=%async_computation.2 | async-start | bytes 131072 | tf_op jit(solution)/shard_map/all_to_all | solution.py:110
Sparse Core Ops, SparseCore 0:
  51.3 20.5 reduce-scatter.1
where the time goes:
time: 94.8 us; the launch traced here: 94.1 us
  waiting for transfers between devices  26.9 us (28%)
  blocking collectives  26.8 us (28%)
  between operations  14.9 us (16%)
  matrix products  10.2 us (11%)
  other arithmetic  6.35 us (7%)
  starting transfers between devices  5.55 us (6%)
  local copies, waits for them, and re-layouts  3.52 us (4%)
    reduce_scatter x1, waiting for transfers between devices, shards(): lax.psum_scatter(partial_value, 'tp', scatter_dimension=3, tiled=True)  20.7 us
    all_to_all x1, blocking collectives, shards(): lax.all_to_all(outbound, 'ep', split_axis=0, concat_axis=0, tiled=True)  13.9 us
    psum x1, blocking collectives, shards(): summed = lax.psum(head_part, 'tp').astype(jnp.float32)  12.9 us
    all_to_all x1, waiting for transfers between devices, shards(): lax.all_to_all(reduced, 'ep', split_axis=0, concat_axis=0, tiled=True)  6.19 us
    all_to_all x1, starting transfers between devices, shards(): lax.all_to_all(reduced, 'ep', split_axis=0, concat_axis=0, tiled=True)  5.52 us
    dot_general x3, matrix products, shards(): jnp.dot(normed, weight, preferred_element_type=jnp.float32)  3.27 us
    dot_general x1, matrix products, shards(): jnp.dot(mixed, w_out, preferred_element_type=jnp.float32)  1.96 us
  transfers between devices with their start and end apart: 2, of which 2 were waited for; matrix products, arithmetic and copies ran while one was open for 1% of the time, Pallas kernels for 0%

commit v1 on v0

v1 whole, which is shorter than its diff:
```python
import functools
import math

import jax
import jax.numpy as jnp
from jax import lax
from jax.experimental import pallas as pl
from jax.experimental.pallas import tpu as pltpu
from jax.sharding import PartitionSpec as P

MESH = pl.DeviceIdType.MESH
F32 = jnp.float32
BF16 = jnp.bfloat16


def kernel(
    n_ep,
    n_tp,
    tokens_h,
    gain_mix_h,
    wq_h,
    wk_h,
    wv_h,
    wo_h,
    wi_h,
    wf_h,
    bias_h,
    w_out_h,
    gain_moe_h,
    memory_h,
    normalizer_h,
    stabilizer_h,
    gate_h,
    up_h,
    down_h,
    routes_h,
    weight_h,
    out_ref,
    memory_out,
    norm_out,
    stab_out,
    tokens,
    gain_mix,
    wq,
    wk,
    wv,
    wo,
    wi,
    wf,
    bias,
    w_out,
    gain_moe,
    memory,
    normalizer,
    stabilizer,
    gate,
    up,
    down,
    routes,
    weight,
    memory_next,
    send1,
    recv1,
    recv2,
    send3,
    recv3,
    in_sems,
    out_sem,
    send_sems,
    recv_sems,
):
    rows, width = tokens.shape
    head_size = wq.shape[1]
    quarter = width // n_tp
    n = n_ep * n_tp
    me_e = lax.axis_index("ep")
    me_t = lax.axis_index("tp")
    me = me_e * n_tp + me_t

    sources = (
        tokens_h, gain_mix_h, wq_h, wk_h, wi_h, wf_h, bias_h, stabilizer_h, wv_h, wo_h,
        memory_h, normalizer_h, w_out_h, gain_moe_h, gate_h, up_h, down_h, routes_h, weight_h,
    )
    targets = (
        tokens, gain_mix, wq, wk, wi, wf, bias, stabilizer, wv, wo,
        memory, normalizer, w_out, gain_moe, gate, up, down, routes, weight,
    )
    copies = {}
    for number, (source, target) in enumerate(zip(sources, targets)):
        copy = pltpu.make_async_copy(source, target, in_sems.at[number])
        copy.start()
        copies[id(target)] = copy

    def ready(*refs):
        for ref in refs:
            copies[id(ref)].wait()

    barrier = pltpu.get_barrier_semaphore()

    def greet(step, carry):
        peer = lax.rem(me + step, n)
        pl.semaphore_signal(
            barrier, inc=1, device_id=(peer // n_tp, lax.rem(peer, n_tp)), device_id_type=MESH
        )
        return carry

    lax.fori_loop(1, n, greet, 0)

    ready(tokens, gain_mix)
    values = tokens[...].astype(F32)
    centered = values - jnp.mean(values, -1, keepdims=True)
    variance = jnp.mean(centered * centered, -1, keepdims=True)
    normed = (centered * lax.rsqrt(variance + 1e-05) * gain_mix[...]).astype(BF16)

    def project(ref):
        ready(ref)
        return jnp.dot(normed, ref[...], preferred_element_type=F32).astype(BF16).astype(F32)

    q = project(wq)
    k = project(wk) / math.sqrt(head_size)
    q_cols = q.T
    k_cols = k.T
    ready(wi, wf, bias, stabilizer)
    normed_wide = normed.astype(F32)
    gate_in = jnp.sum(normed_wide * wi[...].astype(F32), -1, keepdims=True)
    gate_forget = jnp.sum(normed_wide * wf[...].astype(F32), -1, keepdims=True)
    biased = gate_forget + bias[...]
    log_forget = jnp.minimum(biased, 0.0) - jnp.log1p(jnp.exp(-jnp.abs(biased)))
    shifted = log_forget + stabilizer[...]
    stab_next = jnp.maximum(shifted, gate_in)
    keep = jnp.exp(shifted - stab_next)
    admit = jnp.exp(gate_in - stab_next)
    v = project(wv)
    o = project(wo)
    ready(memory)
    read = jnp.concatenate(
        [
            jnp.sum(q_cols[:, s : s + 1] * memory[s, 0], axis=0, keepdims=True)
            for s in range(rows)
        ],
        axis=0,
    )
    numerator = keep * read + (admit * jnp.sum(q * k, -1, keepdims=True)) * v
    ready(normalizer)
    norm_next = keep * normalizer[...].reshape(rows, head_size) + admit * k
    denominator = jnp.sum(q * norm_next, -1, keepdims=True)
    readout = numerator / jnp.maximum(jnp.abs(denominator), jnp.exp(-stab_next))
    mixed = (jax.nn.sigmoid(o) * readout).astype(BF16)
    ready(w_out)
    part = jnp.dot(mixed, w_out[...], preferred_element_type=F32)
    for t in range(n_tp):
        send1[t] = part[:, t * quarter : (t + 1) * quarter].astype(BF16)

    pl.semaphore_wait(barrier, n - 1)
    for step in range(1, n_tp):
        peer = lax.rem(me_t + step, n_tp)
        pltpu.make_async_remote_copy(
            src_ref=send1.at[peer],
            dst_ref=recv1.at[me_t],
            send_sem=send_sems.at[0],
            recv_sem=recv_sems.at[0],
            device_id=(me_e, peer),
            device_id_type=MESH,
        ).start()

    norm_out[...] = norm_next.reshape(norm_out.shape)
    stab_out[...] = stab_next
    scaled_cols = k_cols
    for s in range(rows):
        memory_next[s, 0] = keep[s : s + 1] * memory[s, 0] + scaled_cols[:, s : s + 1] * (
            admit[s : s + 1] * v[s : s + 1]
        )
    state_copy = pltpu.make_async_copy(memory_next, memory_out, out_sem)
    state_copy.start()

    def arrived(ref, count, sem):
        pltpu.make_async_copy(ref.at[pl.ds(0, count)], ref.at[pl.ds(0, count)], sem).wait()

    arrived(recv1, n_tp - 1, recv_sems.at[0])
    own = tokens[:, pl.ds(pl.multiple_of(me_t * quarter, quarter), quarter)].astype(F32)
    own = own + send1[me_t].astype(F32)
    for step in range(1, n_tp):
        own = own + recv1[lax.rem(me_t + step, n_tp)].astype(F32)

    recv2[me] = own.astype(BF16)

    def spread(step, carry):
        peer = lax.rem(me + step, n)
        pltpu.make_async_remote_copy(
            src_ref=recv2.at[me],
            dst_ref=recv2.at[me],
            send_sem=send_sems.at[1],
            recv_sem=recv_sems.at[1],
            device_id=(peer // n_tp, lax.rem(peer, n_tp)),
            device_id_type=MESH,
        ).start()
        return carry

    lax.fori_loop(1, n, spread, 0)
    ready(gain_moe, gate, up, down, routes, weight)
    arrived(recv2, n - 1, recv_sems.at[1])

    group = math.gcd(n_ep, 8)
    tall = group * rows

    def expert(index, carry):
        first = index * group
        pieces = []
        for t in range(n_tp):
            piece = jnp.concatenate(
                [recv2[(first + i) * n_tp + t].astype(F32) for i in range(group)], axis=0
            )
            pieces.append(piece)
        mean = sum(jnp.sum(piece, -1, keepdims=True) for piece in pieces) / width
        pieces = [piece - mean for piece in pieces]
        spreads = sum(jnp.sum(piece * piece, -1, keepdims=True) for piece in pieces) / width
        scale = lax.rsqrt(spreads + 1e-05)
        gate_part = jnp.zeros((tall, gate.shape[2]), F32)
        up_part = jnp.zeros((tall, up.shape[2]), F32)
        for t in range(n_tp):
            cut = slice(t * quarter, (t + 1) * quarter)
            rows_in = (pieces[t] * scale * gain_moe[:, cut]).astype(BF16)
            gate_part += jnp.dot(rows_in, gate[0, cut, :], preferred_element_type=F32)
            up_part += jnp.dot(rows_in, up[0, cut, :], preferred_element_type=F32)
        hidden = (jax.nn.silu(gate_part) * up_part).astype(BF16)
        for t in range(n_tp):
            cut = slice(t * quarter, (t + 1) * quarter)
            partial = jnp.dot(hidden, down[0, :, cut], preferred_element_type=F32)
            for i in range(group):
                send3[(first + i) * n_tp + t] = partial[i * rows : (i + 1) * rows].astype(BF16)
        return carry

    if n_ep == group:
        expert(0, 0)
    else:
        lax.fori_loop(0, n_ep // group, expert, 0)

    def home(step, carry):
        peer = lax.rem(me + step, n)
        pltpu.make_async_remote_copy(
            src_ref=send3.at[peer],
            dst_ref=recv3.at[me],
            send_sem=send_sems.at[2],
            recv_sem=recv_sems.at[2],
            device_id=(peer // n_tp, lax.rem(peer, n_tp)),
            device_id_type=MESH,
        ).start()
        return carry

    lax.fori_loop(1, n, home, 0)
    recv3[me] = send3[me]
    arrived(recv3, n - 1, recv_sems.at[2])
    chosen = routes[...]
    shares = weight[...]

    def add_expert(e, total):
        factor = jnp.sum(jnp.where(chosen == e, shares, 0.0), -1, keepdims=True)
        summed = recv3[e * n_tp].astype(F32)
        for t in range(1, n_tp):
            summed = summed + recv3[e * n_tp + t].astype(F32)
        return total + factor * summed

    if n_ep == group:
        for e in range(n_ep):
            own = add_expert(e, own)
    else:
        own = lax.fori_loop(0, n_ep, add_expert, own)
    out_ref[...] = own.astype(BF16)

    arrived(send1, n_tp - 1, send_sems.at[0])
    arrived(recv2, n - 1, send_sems.at[1])
    arrived(send3, n - 1, send_sems.at[2])
    state_copy.wait()


def shards(
    n_ep,
    n_tp,
    tokens,
    w_query,
    w_key,
    w_value,
    w_outgate,
    w_igate,
    w_fgate,
    forget_bias,
    w_out,
    gain_mix,
    gain_moe,
    memory,
    normalizer,
    stabilizer,
    expert_gate,
    expert_up,
    expert_down,
    routes,
    route_weight,
):
    rows, width = tokens.shape
    n = n_ep * n_tp
    quarter = width // n_tp
    assert memory.shape[1] == 1 and expert_gate.shape[0] == 1
    operands = (
        tokens,
        gain_mix.reshape(1, width),
        w_query,
        w_key,
        w_value,
        w_outgate,
        w_igate.reshape(1, width),
        w_fgate.reshape(1, width),
        forget_bias.reshape(1, 1),
        w_out,
        gain_moe.reshape(1, width),
        memory,
        normalizer,
        stabilizer,
        expert_gate,
        expert_up,
        expert_down,
        routes,
        route_weight,
    )
    block = (n, rows, quarter)
    return pl.pallas_call(
        functools.partial(kernel, n_ep, n_tp),
        out_shape=(
            jax.ShapeDtypeStruct((rows, quarter), BF16),
            jax.ShapeDtypeStruct(memory.shape, F32),
            jax.ShapeDtypeStruct(normalizer.shape, F32),
            jax.ShapeDtypeStruct(stabilizer.shape, F32),
        ),
        in_specs=[pl.BlockSpec(memory_space=pl.ANY)] * len(operands),
        out_specs=(
            pl.BlockSpec(memory_space=pltpu.VMEM),
            pl.BlockSpec(memory_space=pl.ANY),
            pl.BlockSpec(memory_space=pltpu.VMEM),
            pl.BlockSpec(memory_space=pltpu.VMEM),
        ),
        scratch_shapes=[pltpu.VMEM(x.shape, x.dtype) for x in operands]
        + [
            pltpu.VMEM(memory.shape, F32),
            pltpu.VMEM((n_tp, rows, quarter), BF16),
            pltpu.VMEM((n_tp, rows, quarter), BF16),
            pltpu.VMEM(block, BF16),
            pltpu.VMEM(block, BF16),
            pltpu.VMEM(block, BF16),
            pltpu.SemaphoreType.DMA((len(operands),)),
            pltpu.SemaphoreType.DMA,
            pltpu.SemaphoreType.DMA((3,)),
            pltpu.SemaphoreType.DMA((3,)),
        ],
        compiler_params=pltpu.CompilerParams(collective_id=0, has_side_effects=True),
        name="cell_and_experts",
    )(*operands)


def solution(mesh):
    return jax.shard_map(
        functools.partial(shards, mesh.shape["ep"], mesh.shape["tp"]),
        mesh=mesh,
        in_specs=(
            P("ep", None),
            P(None, "tp"),
            P(None, "tp"),
            P(None, "tp"),
            P(None, "tp"),
            P(None, "tp"),
            P(None, "tp"),
            P("tp"),
            P("tp", None),
            P(),
            P(),
            P("ep", "tp", None, None),
            P("ep", "tp", None),
            P("ep", "tp"),
            P("ep", None, "tp"),
            P("ep", None, "tp"),
            P("ep", "tp", None),
            P("ep", None),
            P("ep", None),
        ),
        out_specs=(P("ep", "tp"), P("ep", "tp", None, None), P("ep", "tp", None), P("ep", "tp")),
        check_vma=False,
    )
```

time: 94.8 us -> 37.2 us (0.39)
  the two profiles are of different devices: /device:TPU:0 before, /device:TPU:29 now
where the time goes in v1:
time: 37.2 us; the launch traced here: 36.8 us
  Pallas kernels  25.3 us (68%)
  local copies, waits for them, and re-layouts  10.2 us (27%)
  between operations  1.29 us (3%)
    pallas_call x1, Pallas kernels, shards(): pl.pallas_call(functools.partial(kernel, n_ep, n_tp), out_shape=(jax.Shap...  25.3 us
    unnamed x8, local copies, waits for them, and re-layouts  8.97 us
    pallas_call x1, local copies, waits for them, and re-layouts, shards(): pl.pallas_call(functools.partial(kernel, n_ep, n_tp), out_shape=(jax.Shap...  1.27 us

profile of v1, /device:TPU:29, one launch (start us, length us, event | category | flops | bytes accessed | tf_op | source)
XLA Modules:
  0.0 36.8 jit_solution(4966856391022423464)
XLA Ops:
  1.3 1.3 %copy.23.stabilizer_h = f32[8,1]{1,0:T(8,128)} copy(f32[8,1]{0,1:T(1,128)} %param.32) | data formatting | bytes 64 | tf_op args[13]
  2.6 1.3 %copy.24.routes_h = s32[8,4]{1,0:T(8,128)} copy(s32[8,4]{0,1:T(4,128)} %param.36) | data formatting | bytes 256 | tf_op args[17]
  3.9 1.3 %copy.25.weight_h = f32[8,4]{1,0:T(8,128)} copy(f32[8,4]{0,1:T(4,128)} %param.37) | data formatting | bytes 256 | tf_op args[18]
  5.3 25.3 %cell_and_experts.1 = (bf16[8,512]{1,0:T(8,128)(2,1)}, f32[8,1,256,256]{3,2,1,0:T(8,128)}, f32[8,1,256]{2,1,0:T(1,128)}, f32[8,1]{1,0:T(8,128)}) custom-call(bf16[8,2048]{1,0:T(8,128)(2,1)} %tokens_h.1, f32[1,2048]{1,0:T(1,128)} %bitcast.6, bf16[2048,256]{1,0:T(8,128)(2,1)} %wq_h.1, bf16[2048,256]{1,0:T(8,128)(2,1)} %wk_h.1, bf16[2048,256]{1,0:T(8,128)(2,1)} %wv_h.1, ...), custom_call_target="tpu_custom_call" | custom-call | tf_op jit(solution)/shard_map/cell_and_experts/pallas_call | solution.py:325
  30.6 1.3 %copy.26 = f32[8,1]{0,1:T(1,128)} copy(f32[8,1]{1,0:T(8,128)} %get-tuple-element.7) | data formatting | bytes 64 | tf_op jit(solution)/shard_map/cell_and_experts/pallas_call | solution.py:325
  31.9 1.3 %copy.31 = bf16[8,512]{1,0:T(8,128)(2,1)} copy(bf16[8,512]{1,0:T(8,128)(2,1)} %get-tuple-element.12) | data formatting | bytes 16384
  33.2 0.0 copy-start
  33.2 3.1 %copy.32 = f32[8,1,256,256]{3,2,1,0:T(8,128)} copy(f32[8,1,256,256]{3,2,1,0:T(8,128)} %get-tuple-element.13) | data formatting | bytes 4194304
  36.2 0.0 copy-done
  36.2 0.6 %copy.33 = f32[8,1,256]{2,1,0:T(1,128)} copy(f32[8,1,256]{2,1,0:T(1,128)S(1)} %copy-done) | data formatting | bytes 16384
Async XLA Ops:
  33.2 3.1 %copy-start = (f32[8,1,256]{2,1,0:T(1,128)S(1)}, f32[8,1,256]{2,1,0:T(1,128)}, u32[]{:S(2)}) copy-start(f32[8,1,256]{2,1,0:T(1,128)} %get-tuple-element.14) | copy-start | bytes 24580

commit v2 on v1

--- a/solution.py
+++ b/solution.py
@@ -35,10 +35,7 @@
     down_h,
     routes_h,
     weight_h,
-    out_ref,
-    memory_out,
-    norm_out,
-    stab_out,
+    pack_ref,
     tokens,
     gain_mix,
     wq,
@@ -47,7 +44,6 @@
     wo,
     wi,
     wf,
-    bias,
     w_out,
     gain_moe,
     memory,
@@ -58,31 +54,47 @@
     down,
     routes,
     weight,
-    memory_next,
     send1,
     recv1,
     recv2,
+    give,
+    take,
+    held,
     send3,
     recv3,
     in_sems,
-    out_sem,
     send_sems,
     recv_sems,
 ):
     rows, width = tokens.shape
     head_size = wq.shape[1]
+    diagonal = lax.broadcasted_iota(jnp.int32, (rows, rows), 0) == lax.broadcasted_iota(
+        jnp.int32, (rows, rows), 1
+    )
+
+    def upright(row):
+        return jnp.sum(jnp.where(diagonal, row, 0.0), axis=1, keepdims=True)
+
+    def flat(column):
+        return jnp.sum(jnp.where(diagonal, column, 0.0), axis=0, keepdims=True)
+
     quarter = width // n_tp
     n = n_ep * n_tp
     me_e = lax.axis_index("ep")
     me_t = lax.axis_index("tp")
     me = me_e * n_tp + me_t
+    pairs = n_tp // 2
+    half = n_ep * pairs
+    parity = lax.rem(me_t, 2)
+    mine = me_e * pairs + me_t // 2
+    sibling = (me_e, me_t + 1 - 2 * parity)
 
     sources = (
-        tokens_h, gain_mix_h, wq_h, wk_h, wi_h, wf_h, bias_h, stabilizer_h, wv_h, wo_h,
+        tokens_h, gain_mix_h, wq_h, wk_h, wi_h, wf_h, stabilizer_h, wv_h, wo_h,
         memory_h, normalizer_h, w_out_h, gain_moe_h, gate_h, up_h, down_h, routes_h, weight_h,
     )
     targets = (
-        tokens, gain_mix, wq, wk, wi, wf, bias, stabilizer, wv, wo,
+        tokens, gain_mix, wq, wk, wi, wf, stabilizer, wv, wo,
         memory, normalizer, w_out, gain_moe, gate, up, down, routes, weight,
     )
     copies = {}
@@ -119,14 +131,13 @@
     q = project(wq)
     k = project(wk) / math.sqrt(head_size)
     q_cols = q.T
-    k_cols = k.T
-    ready(wi, wf, bias, stabilizer)
+    ready(wi, wf, stabilizer)
     normed_wide = normed.astype(F32)
     gate_in = jnp.sum(normed_wide * wi[...].astype(F32), -1, keepdims=True)
     gate_forget = jnp.sum(normed_wide * wf[...].astype(F32), -1, keepdims=True)
-    biased = gate_forget + bias[...]
+    biased = gate_forget + bias_h[0]
     log_forget = jnp.minimum(biased, 0.0) - jnp.log1p(jnp.exp(-jnp.abs(biased)))
-    shifted = log_forget + stabilizer[...]
+    shifted = log_forget + upright(stabilizer[...])
     stab_next = jnp.maximum(shifted, gate_in)
     keep = jnp.exp(shifted - stab_next)
     admit = jnp.exp(gate_in - stab_next)
@@ -163,15 +174,12 @@
             device_id_type=MESH,
         ).start()
 
-    norm_out[...] = norm_next.reshape(norm_out.shape)
-    stab_out[...] = stab_next
-    scaled_cols = k_cols
-    for s in range(rows):
-        memory_next[s, 0] = keep[s : s + 1] * memory[s, 0] + scaled_cols[:, s : s + 1] * (
-            admit[s : s + 1] * v[s : s + 1]
-        )
-    state_copy = pltpu.make_async_copy(memory_next, memory_out, out_sem)
-    state_copy.start()
+    lanes = pack_ref.shape[1] - quarter - 3 * head_size
+    pack_ref[:, quarter : quarter + head_size] = admit * k
+    pack_ref[:, quarter + head_size : quarter + 2 * head_size] = v
+    pack_ref[:, quarter + 2 * head_size : quarter + 3 * head_size] = norm_next
+    place = lax.broadcasted_iota(jnp.int32, (rows, lanes), 1)
+    pack_ref[:, quarter + 3 * head_size :] = jnp.where(place == 0, keep, stab_next)
 
     def arrived(ref, count, sem):
         pltpu.make_async_copy(ref.at[pl.ds(0, count)], ref.at[pl.ds(0, count)], sem).wait()
@@ -182,33 +190,51 @@
     for step in range(1, n_tp):
         own = own + recv1[lax.rem(me_t + step, n_tp)].astype(F32)
 
-    recv2[me] = own.astype(BF16)
+    recv2[parity * half + mine] = own.astype(BF16)
 
     def spread(step, carry):
-        peer = lax.rem(me + step, n)
+        other = lax.rem(mine + step, half)
         pltpu.make_async_remote_copy(
-            src_ref=recv2.at[me],
-            dst_ref=recv2.at[me],
+            src_ref=recv2.at[parity * half + mine],
+            dst_ref=recv2.at[parity * half + mine],
             send_sem=send_sems.at[1],
             recv_sem=recv_sems.at[1],
-            device_id=(peer // n_tp, lax.rem(peer, n_tp)),
+            device_id=(other // pairs, lax.rem(other, pairs) * 2 + parity),
             device_id_type=MESH,
         ).start()
         return carry
 
-    lax.fori_loop(1, n, spread, 0)
+    lax.fori_loop(1, half, spread, 0)
     ready(gain_moe, gate, up, down, routes, weight)
-    arrived(recv2, n - 1, recv_sems.at[1])
+    arrived(recv2, half - 1, recv_sems.at[1])
+    pltpu.make_async_remote_copy(
+        src_ref=recv2.at[pl.ds(parity * half, half)],
+        dst_ref=recv2.at[pl.ds(parity * half, half)],
+        send_sem=send_sems.at[3],
+        recv_sem=recv_sems.at[3],
+        device_id=sibling,
+        device_id_type=MESH,
+    ).start()
+    arrived(recv2, half, recv_sems.at[3])
 
     group = math.gcd(n_ep, 8)
     tall = group * rows
+
+    hand = pltpu.make_async_remote_copy(
+        src_ref=give,
+        dst_ref=take,
+        send_sem=send_sems.at[4],
+        recv_sem=recv_sems.at[4],
+        device_id=sibling,
+        device_id_type=MESH,
+    )
 
     def expert(index, carry):
         first = index * group
         pieces = []
         for t in range(n_tp):
             piece = jnp.concatenate(
-                [recv2[(first + i) * n_tp + t].astype(F32) for i in range(group)], axis=0
+                [recv2[(t % 2) * half + (first + i) * pairs + t // 2].astype(F32) for i in range(group)], axis=0
             )
             pieces.append(piece)
         mean = sum(jnp.sum(piece, -1, keepdims=True) for piece in pieces) / width
@@ -223,41 +249,60 @@
             gate_part += jnp.dot(rows_in, gate[0, cut, :], preferred_element_type=F32)
             up_part += jnp.dot(rows_in, up[0, cut, :], preferred_element_type=F32)
         hidden = (jax.nn.silu(gate_part) * up_part).astype(BF16)
-        for t in range(n_tp):
-            cut = slice(t * quarter, (t + 1) * quarter)
-            partial = jnp.dot(hidden, down[0, :, cut], preferred_element_type=F32)
+
+        def partial(t):
+            cut = pl.ds(pl.multiple_of(t * quarter, quarter), quarter)
+            return jnp.dot(hidden, down[0, :, cut], preferred_element_type=F32)
+
+        for j in range(pairs):
+            block = partial(2 * j + 1 - parity)
             for i in range(group):
-                send3[(first + i) * n_tp + t] = partial[i * rows : (i + 1) * rows].astype(BF16)
+                give[(first + i) * pairs + j] = block[i * rows : (i + 1) * rows].astype(BF16)
+        if n_ep == group:
+            hand.start()
+        for j in range(pairs):
+            block = partial(2 * j + parity)
+            for i in range(group):
+                held[(first + i) * pairs + j] = block[i * rows : (i + 1) * rows]
         return carry
 
     if n_ep == group:
         expert(0, 0)
     else:
         lax.fori_loop(0, n_ep // group, expert, 0)
+        hand.start()
+
+    arrived(take, half, recv_sems.at[4])
+
+    def pair_sum(index, carry):
+        send3[index] = (held[index] + take[index].astype(F32)).astype(BF16)
+        return carry
+
+    lax.fori_loop(0, half, pair_sum, 0, unroll=half <= 16)
 
     def home(step, carry):
-        peer = lax.rem(me + step, n)
+        other = lax.rem(mine + step, half)
         pltpu.make_async_remote_copy(
-            src_ref=send3.at[peer],
-            dst_ref=recv3.at[me],
+            src_ref=send3.at[other],
+            dst_ref=recv3.at[mine],
             send_sem=send_sems.at[2],
             recv_sem=recv_sems.at[2],
-            device_id=(peer // n_tp, lax.rem(peer, n_tp)),
+            device_id=(other // pairs, lax.rem(other, pairs) * 2 + parity),
             device_id_type=MESH,
         ).start()
         return carry
 
-    lax.fori_loop(1, n, home, 0)
-    recv3[me] = send3[me]
-    arrived(recv3, n - 1, recv_sems.at[2])
+    lax.fori_loop(1, half, home, 0)
+    recv3[mine] = send3[mine]
+    arrived(recv3, half - 1, recv_sems.at[2])
     chosen = routes[...]
     shares = weight[...]
 
     def add_expert(e, total):
-        factor = jnp.sum(jnp.where(chosen == e, shares, 0.0), -1, keepdims=True)
-        summed = recv3[e * n_tp].astype(F32)
-        for t in range(1, n_tp):
-            summed = summed + recv3[e * n_tp + t].astype(F32)
+        factor = upright(jnp.sum(jnp.where(chosen == e, shares, 0.0), 0, keepdims=True))
+        summed = recv3[e * pairs].astype(F32)
+        for j in range(1, pairs):
+            summed = summed + recv3[e * pairs + j].astype(F32)
         return total + factor * summed
 
     if n_ep == group:
@@ -265,12 +310,50 @@
             own = add_expert(e, own)
     else:
         own = lax.fori_loop(0, n_ep, add_expert, own)
-    out_ref[...] = own.astype(BF16)
+    pack_ref[:, :quarter] = own
 
     arrived(send1, n_tp - 1, send_sems.at[0])
-    arrived(recv2, n - 1, send_sems.at[1])
-    arrived(send3, n - 1, send_sems.at[2])
-    state_copy.wait()
+    arrived(recv2, half - 1, send_sems.at[1])
+    arrived(send3, half - 1, send_sems.at[2])
+    arrived(recv2, half, send_sems.at[3])
+    arrived(give, half, send_sems.at[4])
+
+
+def finish(pack_h, memory_h, out_h, memory_out, norm_out, stab_out, pack, memory, out, norm, stab, in_sems, out_sems):
+    count = memory.shape[0]
+    rows, quarter = out.shape
+    head_size = memory.shape[2]
+    first = pltpu.make_async_copy(pack_h, pack, in_sems.at[count])
+    first.start()
+    reads = [pltpu.make_async_copy(memory_h.at[s], memory.at[s], in_sems.at[s]) for s in range(count)]
+    for read in reads:
+        read.start()
+    first.wait()
+    out[...] = pack[:, :quarter].astype(BF16)
+    norm[...] = pack[:, quarter + 2 * head_size : quarter + 3 * head_size].reshape(norm.shape)
+    diagonal = lax.broadcasted_iota(jnp.int32, (rows, rows), 0) == lax.broadcasted_iota(
+        jnp.int32, (rows, rows), 1
+    )
+    base = quarter + 3 * head_size
+    stab[...] = jnp.sum(jnp.where(diagonal, pack[:, base + 1 : base + 2], 0.0), axis=0, keepdims=True)
+    writes = [
+        pltpu.make_async_copy(out, out_h, out_sems.at[count]),
+        pltpu.make_async_copy(norm, norm_out, out_sems.at[count + 1]),
+        pltpu.make_async_copy(stab, stab_out, out_sems.at[count + 2]),
+    ]
+    for write in writes:
+        write.start()
+    k_cols = pack[:, quarter : quarter + head_size].T
+    v = pack[:, quarter + head_size : quarter + 2 * head_size]
+    keep = pack[:, base : base + 1]
+    for s in range(count):
+        reads[s].wait()
+        memory[s, 0] = keep[s : s + 1] * memory[s, 0] + k_cols[:, s : s + 1] * v[s : s + 1]
+        write = pltpu.make_async_copy(memory.at[s], memory_out.at[s], out_sems.at[s])
+        write.start()
+        writes.append(write)
+    for write in writes:
+        write.wait()
 
 
 def shards(
@@ -309,50 +392,69 @@
         w_outgate,
         w_igate.reshape(1, width),
         w_fgate.reshape(1, width),
-        forget_bias.reshape(1, 1),
+        forget_bias,
         w_out,
         gain_moe.reshape(1, width),
         memory,
         normalizer,
-        stabilizer,
+        stabilizer.T,
         expert_gate,
         expert_up,
         expert_down,
-        routes,
-        route_weight,
+        routes.T,
+        route_weight.T,
     )
     block = (n, rows, quarter)
-    return pl.pallas_call(
+    half = (n // 2, rows, quarter)
+    head_size = memory.shape[2]
+    pack_width = quarter + 3 * head_size + 128
+    pack = pl.pallas_call(
         functools.partial(kernel, n_ep, n_tp),
-        out_shape=(
-            jax.ShapeDtypeStruct((rows, quarter), BF16),
-            jax.ShapeDtypeStruct(memory.shape, F32),
-            jax.ShapeDtypeStruct(normalizer.shape, F32),
-            jax.ShapeDtypeStruct(stabilizer.shape, F32),
-        ),
-        in_specs=[pl.BlockSpec(memory_space=pl.ANY)] * len(operands),
-        out_specs=(
-            pl.BlockSpec(memory_space=pltpu.VMEM),
-            pl.BlockSpec(memory_space=pl.ANY),
-            pl.BlockSpec(memory_space=pltpu.VMEM),
-            pl.BlockSpec(memory_space=pltpu.VMEM),
-        ),
-        scratch_shapes=[pltpu.VMEM(x.shape, x.dtype) for x in operands]
+        out_shape=jax.ShapeDtypeStruct((rows, pack_width), F32),
+        in_specs=[
+            pl.BlockSpec(memory_space=pltpu.SMEM if x is forget_bias else pl.ANY) for x in operands
+        ],
+        out_specs=pl.BlockSpec(memory_space=pltpu.VMEM),
+        scratch_shapes=[pltpu.VMEM(x.shape, x.dtype) for x in operands if x is not forget_bias]
         + [
-            pltpu.VMEM(memory.shape, F32),
             pltpu.VMEM((n_tp, rows, quarter), BF16),
             pltpu.VMEM((n_tp, rows, quarter), BF16),
             pltpu.VMEM(block, BF16),
-            pltpu.VMEM(block, BF16),
-            pltpu.VMEM(block, BF16),
+            pltpu.VMEM(half, BF16),
+            pltpu.VMEM(half, BF16),
+            pltpu.VMEM(half, F32),
+            pltpu.VMEM(half, BF16),
+            pltpu.VMEM(half, BF16),
             pltpu.SemaphoreType.DMA((len(operands),)),
-            pltpu.SemaphoreType.DMA,
-            pltpu.SemaphoreType.DMA((3,)),
-            pltpu.SemaphoreType.DMA((3,)),
+            pltpu.SemaphoreType.DMA((5,)),
+            pltpu.SemaphoreType.DMA((5,)),
         ],
         compiler_params=pltpu.CompilerParams(collective_id=0, has_side_effects=True),
         name="cell_and_experts",
     )(*operands)
+    results = (
+        jax.ShapeDtypeStruct((rows, quarter), BF16),
+        jax.ShapeDtypeStruct(memory.shape, F32),
+        jax.ShapeDtypeStruct(normalizer.shape, F32),
+        jax.ShapeDtypeStruct((1, rows), F32),
+    )
+    out, memory_next, norm_next, stab_row = pl.pallas_call(
+        finish,
+        out_shape=results,
+        in_specs=[pl.BlockSpec(memory_space=pl.ANY)] * 2,
+        out_specs=[pl.BlockSpec(memory_space=pl.ANY)] * 4,
+        scratch_shapes=[
+            pltpu.VMEM((rows, pack_width), F32),
+            pltpu.VMEM(memory.shape, F32),
+            pltpu.VMEM((rows, quarter), BF16),
+            pltpu.VMEM(normalizer.shape, F32),
+            pltpu.VMEM((1, rows), F32),
+            pltpu.SemaphoreType.DMA((rows + 1,)),
+            pltpu.SemaphoreType.DMA((rows + 3,)),
+        ],
+        name="state",
+    )(pack, memory)
+    return out, memory_next, norm_next, stab_row.T
 
 
 def solution(mesh):

time: 37.2 us -> 27.8 us (0.75)
  the two profiles are of different devices: /device:TPU:29 before, /device:TPU:0 now
where the time goes in v2:
time: 27.8 us; the launch traced here: 27.7 us
  Pallas kernels  26.4 us (95%)
  between operations  1.29 us (5%)
    pallas_call x1, Pallas kernels, shards(): pl.pallas_call(functools.partial(kernel, n_ep, n_tp), out_shape=jax.Shape...  23.6 us
    pallas_call x1, Pallas kernels, shards(): pl.pallas_call(finish, out_shape=results, in_specs=[pl.BlockSpec(memory_s...  2.74 us

profile of v2, /device:TPU:0, one launch (start us, length us, event | category | flops | bytes accessed | tf_op | source)
XLA Modules:
  0.0 27.7 jit_solution(4013969408361222716)
XLA Ops:
  1.3 23.6 %cell_and_experts.1.pack_h = f32[8,1408]{1,0:T(8,128)} custom-call(bf16[8,2048]{1,0:T(8,128)(2,1)} %tokens_h.1, f32[1,2048]{1,0:T(1,128)} %bitcast.8, bf16[2048,256]{1,0:T(8,128)(2,1)} %wq_h.1, bf16[2048,256]{1,0:T(8,128)(2,1)} %wk_h.1, bf16[2048,256]{1,0:T(8,128)(2,1)} %wv_h.1, bf16[2048,256]{1,0:T(8,128)(2,1)} %wo_h.1, bf16[1,2048]{1,0:T(2,128)(2,1)} %bitcast.9, ...), custom_call_target="tpu_custom_call" | custom-call | tf_op jit(solution)/shard_map/cell_and_experts/pallas_call | solution.py:411
  24.9 2.7 %state.1 = (bf16[8,512]{1,0:T(8,128)(2,1)}, f32[8,1,256,256]{3,2,1,0:T(8,128)}, f32[8,1,256]{2,1,0:T(1,128)}, f32[1,8]{1,0:T(1,128)}) custom-call(f32[8,1408]{1,0:T(8,128)} %cell_and_experts.1.pack_h, f32[8,1,256,256]{3,2,1,0:T(8,128)} %memory_h.3), custom_call_target="tpu_custom_call" | custom-call | tf_op jit(solution)/shard_map/state/pallas_call | solution.py:441
